TPU v7x, 32 devices: a whole 2x2x4 slice. The times are simulated.
32 devices in a mesh: grp: 1, fs: 2 (over x), tp: 16 (over z, y, core).
Axes of the slice: x: 2, y: 2, z: 4, core: 2. Of those that a mesh axis runs over, the one named last changes fastest.
Arguments:
- prompt_rows: bfloat16 [512, 2048], P(('grp', 'fs')), may hold values from -6 to 6
- gain_before: float32 [2048], P('fs'), may hold values from 0.1 to 1.9
- gate_before: float32 [2048, 5632], P('fs', 'tp'), may hold values from -0.125 to 0.125
- up_before: float32 [2048, 5632], P('fs', 'tp'), may hold values from -0.125 to 0.125
- down_before: float32 [5632, 2048], P('fs', 'tp'), may hold values from -0.3125 to 0.3125
- gain_after: float32 [2048], P('fs'), may hold values from 0.1 to 1.9
- gate_after: float32 [2048, 5632], P('fs', 'tp'), may hold values from -0.125 to 0.125
- up_after: float32 [2048, 5632], P('fs', 'tp'), may hold values from -0.125 to 0.125
- down_after: float32 [5632, 2048], P('fs', 'tp'), may hold values from -0.3125 to 0.3125
Outputs:
- mixed_rows: bfloat16 [512, 2048], P(('grp', 'fs'))
- served_gate_before: bfloat16 [2048, 5632], P('grp', 'tp')
- served_up_before: bfloat16 [2048, 5632], P('grp', 'tp')
- served_down_before: bfloat16 [5632, 2048], P(('grp', 'tp'))
- served_gate_after: bfloat16 [2048, 5632], P('grp', 'tp')
- served_up_after: bfloat16 [2048, 5632], P('grp', 'tp')
- served_down_after: bfloat16 [5632, 2048], P(('grp', 'tp'))
All inputs are finite; a program needn't handle non-finite values.
Results may differ from a plain program's by a relative error of at most 0.03.
Values may be sent and summed in bfloat16 or wider, within the bound.
A program may use at most 64 MiB of HBM per device.

v0:
```python
import functools

import jax
import jax.numpy as jnp
from jax import lax
from jax.experimental import pallas as pl
from jax.experimental.pallas import tpu as pltpu
from jax.sharding import PartitionSpec as P

MESH = pl.DeviceIdType.MESH
BF16 = jnp.bfloat16
F32 = jnp.float32

EPS = 1e-06


def serve_weights(gain, gate_w, up_w, down_w):
    gate_half = (gain[:, None] * gate_w).astype(jnp.bfloat16)
    up_half = (gain[:, None] * up_w).astype(jnp.bfloat16)
    down_half = down_w.astype(jnp.bfloat16)
    gate_whole, up_whole = (
        lax.all_gather(gate_half, "fs", axis=0, tiled=True),
        lax.all_gather(up_half, "fs", axis=0, tiled=True),
    )
    tall_block = lax.all_gather(down_half, "fs", axis=0, tiled=True)
    down_whole = lax.all_to_all(tall_block, "tp", split_axis=0, concat_axis=1, tiled=True)
    return (gate_whole, up_whole, down_whole)


def half_step(row_block, gate_w, up_w, down_w):
    values = row_block.astype(jnp.float32)
    normed = (values * lax.rsqrt(jnp.mean(values * values, axis=-1, keepdims=True) + EPS)).astype(
        jnp.bfloat16
    )
    gate_pre = jnp.dot(normed, gate_w, preferred_element_type=jnp.float32)
    up_pre = jnp.dot(normed, up_w, preferred_element_type=jnp.float32)
    hidden = (jax.nn.silu(gate_pre) * up_pre).astype(jnp.bfloat16)
    total = lax.psum(
        jnp.dot(hidden, down_w, preferred_element_type=jnp.float32).astype(jnp.bfloat16), "tp"
    ).astype(jnp.float32)
    return (values + 0.5 * total).astype(jnp.bfloat16)


def body(
    prompt_rows,
    gain_before,
    gate_before,
    up_before,
    down_before,
    gain_after,
    gate_after,
    up_after,
    down_after,
):
    gate_one, up_one, down_one = serve_weights(gain_before, gate_before, up_before, down_before)
    gate_two, up_two, down_two = serve_weights(gain_after, gate_after, up_after, down_after)
    middle = half_step(prompt_rows, gate_one, up_one, down_one)
    mixed = half_step(middle, gate_two, up_two, down_two)
    return (mixed, gate_one, up_one, down_one, gate_two, up_two, down_two)


def rows_of(start, size, unit):
    return pl.ds(pl.multiple_of(start, unit), size)


def kernel(
    n_tp,
    x_hbm, gain1_hbm, gate1_hbm, up1_hbm, down1_hbm, gain2_hbm, gate2_hbm, up2_hbm, down2_hbm,
    mixed_hbm, gate1_out, up1_out, down1_out, gate2_out, up2_out, down2_out,
    x, gain, wide, tall_in, served, tall, down, normed, hidden, part, pair, half, scatter, rows_out,
    in_sem, out_sem, x_send, x_recv, a_send, a_recv, p_send, p_recv, s_send, s_recv, g_send, g_recv,
    h_send, h_recv,
):
    f = lax.axis_index("fs")
    t = lax.axis_index("tp")
    other = 1 - f
    core = lax.rem(t, 2)
    chip = t // 2
    sibling = t + 1 - 2 * core
    chips = n_tp // 2
    width, depth = wide.shape[1:]
    tall_half = tall_in.shape[1]
    block = down.shape[1]
    col = tall.shape[2]
    tokens = x.shape[0]
    side = tokens // 2
    piece = side // chips
    per_half = n_tp // 2

    loads = {}
    sources = (
        ("down1", down1_hbm, tall_in.at[0]), ("gain1", gain1_hbm, gain.at[0]),
        ("gate1", gate1_hbm, wide.at[0]), ("up1", up1_hbm, wide.at[1]),
        ("down2", down2_hbm, tall_in.at[1]), ("gain2", gain2_hbm, gain.at[1]),
        ("gate2", gate2_hbm, wide.at[2]), ("up2", up2_hbm, wide.at[3]), ("x", x_hbm, x),
    )
    for i, (name, src, dst) in enumerate(sources):
        loads[name] = pltpu.make_async_copy(src, dst, in_sem.at[i])
        loads[name].start()

    barrier = pltpu.get_barrier_semaphore()
    for k in range(1, n_tp):
        pl.semaphore_signal(
            barrier, inc=1, device_id={"fs": f, "tp": lax.rem(t + k, n_tp)}, device_id_type=MESH
        )
    pl.semaphore_signal(barrier, inc=1, device_id={"fs": other, "tp": t}, device_id_type=MESH)
    pl.semaphore_wait(barrier, n_tp)

    def across(ref, slot):
        return pltpu.make_async_remote_copy(
            src_ref=ref, dst_ref=ref, send_sem=x_send.at[slot], recv_sem=x_recv.at[slot],
            device_id={"fs": other, "tp": t}, device_id_type=MESH,
        )

    near = rows_of(f * depth, depth, depth)

    def fold_wide(i, gain_slot):
        def one(k, _):
            rows = rows_of(k * 32, 32, 32)
            served[i, rows, near] = (gain[gain_slot] * wide[i, rows, :]).astype(BF16)
            return 0

        lax.fori_loop(0, width // 32, one, 0)
        return across(served.at[i, :, near], i)

    def fold_tall(layer):
        step = tall_half // 8

        def one(k, _):
            tall[layer, rows_of(f * tall_half + k * step, step, 16), :] = tall_in[
                layer, rows_of(k * step, step, 16), :
            ].astype(BF16)
            return 0

        lax.fori_loop(0, 8, one, 0)
        return across(tall.at[layer, rows_of(f * tall_half, tall_half, 16)], 4 + layer)

    my_cols = pl.ds(pl.multiple_of(t * col, col), col)

    def block_copy(layer, b, sender):
        return pltpu.make_async_remote_copy(
            src_ref=tall.at[layer, rows_of(b * block, block, 16)],
            dst_ref=down.at[layer, :, my_cols],
            send_sem=a_send.at[layer, b], recv_sem=a_recv.at[layer, sender],
            device_id={"fs": f, "tp": b}, device_id_type=MESH,
        )

    def hand_out(layer, which):
        def one(k, _):
            b = which * per_half + lax.rem(t + k, per_half)

            @pl.when(b != t)
            def _():
                block_copy(layer, b, t).start()

            return 0

        lax.fori_loop(0, per_half, one, 0)

    def collect(layer):
        def one(k, _):
            block_copy(layer, t, lax.rem(t + k, n_tp)).wait_recv()
            return 0

        lax.fori_loop(1, n_tp, one, 0)
        down[layer, :, my_cols] = tall[layer, rows_of(t * block, block, 16), :]

    outs = []

    def put(src, dst):
        copy = pltpu.make_async_copy(src, dst, out_sem.at[len(outs)])
        copy.start()
        outs.append(copy)

    sends = []
    loads["down1"].wait()
    tall_one = fold_tall(0)
    tall_one.start()
    hand_out(0, f)
    loads["down2"].wait()
    tall_two = fold_tall(1)
    tall_two.start()
    hand_out(1, f)
    loads["gain1"].wait()
    loads["gate1"].wait()
    gate_one = fold_wide(0, 0)
    loads["up1"].wait()
    up_one = fold_wide(1, 0)
    loads["gain2"].wait()
    loads["gate2"].wait()
    gate_two = fold_wide(2, 1)
    loads["up2"].wait()
    up_two = fold_wide(3, 1)
    loads["x"].wait()

    def norm(src):
        def one(k, _):
            rows = rows_of(k * 32, 32, 32)
            v = src[rows, :].astype(F32)
            scale = lax.rsqrt(jnp.mean(v * v, axis=-1, keepdims=True) + EPS)
            normed[rows, :] = (v * scale).astype(BF16)
            return 0

        lax.fori_loop(0, tokens // 32, one, 0)

    norm(x)
    tall_one.wait_recv()
    gate_one.start()
    hand_out(0, other)
    tall_two.wait_recv()
    up_one.start()
    hand_out(1, other)

    turned = (((1,), (1,)), ((), ()))

    def hide(layer):
        gate, up = served.at[2 * layer], served.at[2 * layer + 1]
        step = tokens // 2

        def one(k, _):
            rows = rows_of(k * step, step, step)
            v = normed[rows, :]
            g = lax.dot_general(v, gate[...], turned, preferred_element_type=F32)
            u = lax.dot_general(v, up[...], turned, preferred_element_type=F32)
            hidden[rows, :] = (g / (1.0 + jnp.exp(-g)) * u).astype(BF16)
            return 0

        lax.fori_loop(0, 2, one, 0)

    def project(layer):
        step = tokens // 2

        def one(k, _):
            rows = rows_of(k * step, step, step)
            p = jnp.dot(hidden[rows, :], down[layer], preferred_element_type=F32)
            part[layer, rows, :] = p.astype(BF16)
            return 0

        lax.fori_loop(0, 2, one, 0)

    def chip_copy(src, dst, send, recv, q, sem_at, layer):
        return pltpu.make_async_remote_copy(
            src_ref=src, dst_ref=dst, send_sem=send.at[layer, q], recv_sem=recv.at[layer, sem_at],
            device_id={"fs": f, "tp": 2 * q + core}, device_id_type=MESH,
        )

    def to_sibling(src, dst, send, recv, layer):
        return pltpu.make_async_remote_copy(
            src_ref=src, dst_ref=dst, send_sem=send.at[layer], recv_sem=recv.at[layer],
            device_id={"fs": f, "tp": sibling}, device_id_type=MESH,
        )

    lanes = chips // 2
    lane = lax.rem(chip, 2)
    beside = chip + 1 - 2 * lane

    def place(q):
        return lax.rem(q, 2) * lanes + q // 2

    def scatter_copy(layer, q, sender):
        return chip_copy(
            half.at[layer, rows_of(place(q) * piece, piece, piece)], scatter.at[layer, sender],
            s_send, s_recv, q, sender, layer,
        )

    mine = rows_of(core * side + place(chip) * piece, piece, piece)

    def gather_copy(layer, q, sender):
        ref = rows_out.at[layer, mine]
        return chip_copy(ref, ref, g_send, g_recv, q, sender, layer)

    def for_chips(act):
        def one(k, _):
            act(lax.rem(chip + k, chips))
            return 0

        lax.fori_loop(1, chips, one, 0)

    def for_lane(act):
        def one(k, _):
            act(2 * lax.rem(chip // 2 + k, lanes) + lane)
            return 0

        lax.fori_loop(1, lanes, one, 0)

    def beside_copy(layer, sender):
        ref = rows_out.at[layer, rows_of(core * side + lane * (side // 2), side // 2, side // 2)]
        return chip_copy(ref, ref, g_send, g_recv, beside, sender, layer)

    def add_up(layer, base):
        swap = to_sibling(
            part.at[layer, rows_of((1 - core) * side, side, side)], pair.at[layer], p_send, p_recv, layer
        )
        swap.start()
        swap.wait_recv()

        def add(k, _):
            rows = rows_of(k * piece, piece, piece)
            own = part[layer, rows_of(core * side + k * piece, piece, piece), :].astype(F32)
            half[layer, rows, :] = (own + pair[layer, rows, :].astype(F32)).astype(BF16)
            return 0

        lax.fori_loop(0, chips, add, 0)
        for_chips(lambda q: scatter_copy(layer, q, chip).start())
        for_chips(lambda q: scatter_copy(layer, chip, q).wait_recv())
        scatter[layer, chip] = half[layer, rows_of(place(chip) * piece, piece, piece), :]
        total = scatter[layer, 0].astype(F32)
        for q in range(1, chips):
            total = total + scatter[layer, q].astype(F32)
        rows_out[layer, mine, :] = (base[mine, :].astype(F32) + 0.5 * total).astype(BF16)
        spread = for_chips if layer else for_lane
        spread(lambda q: gather_copy(layer, q, chip).start())
        spread(lambda q: gather_copy(layer, chip, q).wait_recv())
        if layer == 0:
            beside_copy(layer, chip).start()
            beside_copy(layer, beside).wait_recv()
        ref = rows_out.at[layer, rows_of(core * side, side, side)]
        fill = to_sibling(ref, ref, h_send, h_recv, layer)
        fill.start()
        fill.wait_recv()
        sends.extend((swap, fill))

    gate_one.wait_recv()
    gate_two.start()
    put(served.at[0], gate1_out)
    up_one.wait_recv()
    up_two.start()
    put(served.at[1], up1_out)
    hide(0)
    collect(0)
    put(down.at[0], down1_out)
    project(0)
    add_up(0, x)
    norm(rows_out.at[0])
    gate_two.wait_recv()
    up_two.wait_recv()
    put(served.at[2], gate2_out)
    put(served.at[3], up2_out)
    hide(1)
    collect(1)
    put(down.at[1], down2_out)
    project(1)
    add_up(1, rows_out.at[0])
    put(rows_out.at[1], mixed_hbm)

    for sent in (tall_one, gate_one, up_one, tall_two, gate_two, up_two, *sends):
        sent.wait_send()
    for layer in range(2):

        def drain(k, _):
            block_copy(layer, lax.rem(t + k, n_tp), t).wait_send()
            return 0

        lax.fori_loop(1, n_tp, drain, 0)
        for_chips(lambda q: scatter_copy(layer, q, chip).wait_send())
        if layer == 0:
            for_lane(lambda q: gather_copy(layer, q, chip).wait_send())
            beside_copy(layer, chip).wait_send()
        else:
            for_chips(lambda q: gather_copy(layer, q, chip).wait_send())
    for copy in outs:
        copy.wait()


def fused(n_tp, x, gain1, gate1, up1, down1, gain2, gate2, up2, down2):
    depth, width = gate1.shape
    tall_half, col = down1.shape
    tokens, model = x.shape
    block = 2 * tall_half // n_tp
    chips = n_tp // 2
    side = tokens // 2
    dma = pltpu.SemaphoreType.DMA
    shape = jax.ShapeDtypeStruct
    anywhere = pl.BlockSpec(memory_space=pl.ANY)
    wide_out = shape((width, 2 * depth), BF16)
    down_out = shape((block, model), BF16)
    mixed, gate_one, up_one, down_one, gate_two, up_two, down_two = pl.pallas_call(
        functools.partial(kernel, n_tp),
        out_shape=(shape(x.shape, BF16), wide_out, wide_out, down_out, wide_out, wide_out, down_out),
        in_specs=[anywhere] * 9,
        out_specs=[anywhere] * 7,
        scratch_shapes=[
            pltpu.VMEM((tokens, model), BF16),
            pltpu.VMEM((2, 1, depth), F32),
            pltpu.VMEM((4, width, depth), F32),
            pltpu.VMEM((2, tall_half, col), F32),
            pltpu.VMEM((4, width, 2 * depth), BF16),
            pltpu.VMEM((2, 2 * tall_half, col), BF16),
            pltpu.VMEM((2, block, model), BF16),
            pltpu.VMEM((tokens, model), BF16),
            pltpu.VMEM((tokens, width), BF16),
            pltpu.VMEM((2, tokens, model), BF16),
            pltpu.VMEM((2, side, model), BF16),
            pltpu.VMEM((2, side, model), BF16),
            pltpu.VMEM((2, chips, side // chips, model), BF16),
            pltpu.VMEM((2, tokens, model), BF16),
            dma((9,)), dma((7,)), dma((6,)), dma((6,)), dma((2, n_tp)), dma((2, n_tp)),
            dma((2,)), dma((2,)), dma((2, chips)), dma((2, chips)), dma((2, chips)), dma((2, chips)),
            dma((2,)), dma((2,)),
        ],
        compiler_params=pltpu.CompilerParams(
            collective_id=0, has_side_effects=True, vmem_limit_bytes=56 * 1024 * 1024
        ),
        name="hand_over",
    )(x, gain1[None, :], gate1.T, up1.T, down1, gain2[None, :], gate2.T, up2.T, down2)
    return (mixed, gate_one.T, up_one.T, down_one, gate_two.T, up_two.T, down_two)


def solution(mesh):
    placed = (
        P(("grp", "fs"), None),
        P("fs"),
        P("fs", "tp"),
        P("fs", "tp"),
        P("fs", "tp"),
        P("fs"),
        P("fs", "tp"),
        P("fs", "tp"),
        P("fs", "tp"),
    )
    paired = mesh.shape["fs"] == 2 and mesh.shape["tp"] % 4 == 0
    return jax.shard_map(
        functools.partial(fused, mesh.shape["tp"]) if paired else body,
        mesh=mesh,
        in_specs=placed,
        out_specs=(
            P(("grp", "fs"), None),
            P("grp", "tp"),
            P("grp", "tp"),
            P(("grp", "tp"), None),
            P("grp", "tp"),
            P("grp", "tp"),
            P(("grp", "tp"), None),
        ),
        check_vma=False,
    )
```

profile of v0, /device:TPU:0, one launch (start us, length us, event | category | flops | bytes accessed | tf_op | source)
XLA Modules:
  0.0 158.6 jit_solution(91462399750558834)
XLA Ops:
  0.6 145.0 %hand_over.1 = (bf16[256,2048]{1,0:T(8,128)(2,1)}, bf16[352,2048]{1,0:T(8,128)(2,1)}, bf16[352,2048]{1,0:T(8,128)(2,1)}, bf16[352,2048]{1,0:T(8,128)(2,1)}, bf16...) custom-call(bf16[256,2048]{1,0:T(8,128)(2,1)} %x_hbm.1, f32[1,1024]{1,0:T(1,128)} %bitcast.18, ...), custom_call_target="tpu_custom_call" | custom-call | tf_op jit(solution)/shard_map/hand_over/pallas_call | solution.py:377
  145.6 0.0 copy-start.5
  145.6 2.4 %copy.23 = bf16[256,2048]{1,0:T(8,128)(2,1)} copy(bf16[256,2048]{1,0:T(8,128)(2,1)} %get-tuple-element.28) | data formatting | bytes 2097152
  148.1 0.0 copy-done.5
  148.1 0.0 copy-start.4
  148.1 1.1 copy.24
  149.2 0.8 copy-done.4
  149.9 0.0 copy-start.3
  149.9 1.1 copy.25
  151.0 0.8 copy-done.3
  151.8 0.0 copy-start.2
  151.8 1.1 copy.26
  152.9 0.8 copy-done.2
  153.7 0.0 copy-start.1
  153.7 1.1 copy.27
  154.8 0.8 copy-done.1
  155.6 0.0 copy-start
  155.6 1.1 copy.28
  156.7 0.8 copy-done
  157.5 1.1 copy.29
Async XLA Ops:
  145.6 2.4 %copy-start.5 = (bf16[352,2048]{1,0:T(8,128)(2,1)S(1)}, bf16[352,2048]{1,0:T(8,128)(2,1)}, u32[]{:S(2)}) copy-start(bf16[352,2048]{1,0:T(8,128)(2,1)} %get-tuple-element.15) | copy-start | bytes 4325380
  148.1 1.9 %copy-start.4 = (bf16[352,2048]{1,0:T(8,128)(2,1)S(1)}, bf16[352,2048]{1,0:T(8,128)(2,1)}, u32[]{:S(2)}) copy-start(bf16[352,2048]{1,0:T(8,128)(2,1)} %get-tuple-element.16) | copy-start | bytes 4325380
  149.9 1.9 %copy-start.3 = (bf16[352,2048]{1,0:T(8,128)(2,1)S(1)}, bf16[352,2048]{1,0:T(8,128)(2,1)}, u32[]{:S(2)}) copy-start(bf16[352,2048]{1,0:T(8,128)(2,1)} %get-tuple-element.31) | copy-start | bytes 4325380
  151.8 1.9 %copy-start.2 = (bf16[352,2048]{1,0:T(8,128)(2,1)S(1)}, bf16[352,2048]{1,0:T(8,128)(2,1)}, u32[]{:S(2)}) copy-start(bf16[352,2048]{1,0:T(8,128)(2,1)} %get-tuple-element.18) | copy-start | bytes 4325380
  153.7 1.9 %copy-start.1 = (bf16[352,2048]{1,0:T(8,128)(2,1)S(1)}, bf16[352,2048]{1,0:T(8,128)(2,1)}, u32[]{:S(2)}) copy-start(bf16[352,2048]{1,0:T(8,128)(2,1)} %get-tuple-element.19) | copy-start | bytes 4325380
  155.6 1.9 %copy-start = (bf16[352,2048]{1,0:T(8,128)(2,1)S(1)}, bf16[352,2048]{1,0:T(8,128)(2,1)}, u32[]{:S(2)}) copy-start(bf16[352,2048]{1,0:T(8,128)(2,1)} %get-tuple-element.34) | copy-start | bytes 4325380
where the time goes:
time: 161 us; the launch traced here: 159 us
  Pallas kernels  145 us (90%)
  local copies, waits for them, and re-layouts  12.9 us (8%)
    pallas_call x1, Pallas kernels, fused(): pl.pallas_call(functools.partial(kernel, n_tp), out_shape=(shape(x.shape,...  145 us
    unnamed x19, local copies, waits for them, and re-layouts  12.9 us

commit v1 on v0

v1 whole, which is shorter than its diff:
```python
import functools

import jax
import jax.numpy as jnp
from jax import lax
from jax.experimental import pallas as pl
from jax.experimental.pallas import tpu as pltpu
from jax.sharding import PartitionSpec as P

MESH = pl.DeviceIdType.MESH
BF16 = jnp.bfloat16
F32 = jnp.float32

EPS = 1e-06


def serve_weights(gain, gate_w, up_w, down_w):
    gate_half = (gain[:, None] * gate_w).astype(jnp.bfloat16)
    up_half = (gain[:, None] * up_w).astype(jnp.bfloat16)
    down_half = down_w.astype(jnp.bfloat16)
    gate_whole, up_whole = (
        lax.all_gather(gate_half, "fs", axis=0, tiled=True),
        lax.all_gather(up_half, "fs", axis=0, tiled=True),
    )
    tall_block = lax.all_gather(down_half, "fs", axis=0, tiled=True)
    down_whole = lax.all_to_all(tall_block, "tp", split_axis=0, concat_axis=1, tiled=True)
    return (gate_whole, up_whole, down_whole)


def half_step(row_block, gate_w, up_w, down_w):
    values = row_block.astype(jnp.float32)
    normed = (values * lax.rsqrt(jnp.mean(values * values, axis=-1, keepdims=True) + EPS)).astype(
        jnp.bfloat16
    )
    gate_pre = jnp.dot(normed, gate_w, preferred_element_type=jnp.float32)
    up_pre = jnp.dot(normed, up_w, preferred_element_type=jnp.float32)
    hidden = (jax.nn.silu(gate_pre) * up_pre).astype(jnp.bfloat16)
    total = lax.psum(
        jnp.dot(hidden, down_w, preferred_element_type=jnp.float32).astype(jnp.bfloat16), "tp"
    ).astype(jnp.float32)
    return (values + 0.5 * total).astype(jnp.bfloat16)


def body(
    prompt_rows,
    gain_before,
    gate_before,
    up_before,
    down_before,
    gain_after,
    gate_after,
    up_after,
    down_after,
):
    gate_one, up_one, down_one = serve_weights(gain_before, gate_before, up_before, down_before)
    gate_two, up_two, down_two = serve_weights(gain_after, gate_after, up_after, down_after)
    middle = half_step(prompt_rows, gate_one, up_one, down_one)
    mixed = half_step(middle, gate_two, up_two, down_two)
    return (mixed, gate_one, up_one, down_one, gate_two, up_two, down_two)


def rows_of(start, size, unit):
    return pl.ds(pl.multiple_of(start, unit), size)


def kernel(
    n_tp,
    x_hbm, gain1_hbm, gate1_hbm, up1_hbm, down1_hbm, gain2_hbm, gate2_hbm, up2_hbm, down2_hbm,
    mixed, gate1, up1, down1, gate2, up2, down2,
    x, gain, wide, tall_in, tall, normed, hidden, part, pair, ysend, yrecv, zsend, zrecv, middle,
    in_sem, x_send, x_recv, a_send, a_recv, p_send, p_recv, y_send, y_recv, s_send, s_recv,
    g_send, g_recv, b_send, h_send, h_recv,
):
    f = lax.axis_index("fs")
    t = lax.axis_index("tp")
    other = 1 - f
    core = lax.rem(t, 2)
    chip = t // 2
    sibling = t + 1 - 2 * core
    chips = n_tp // 2
    width, depth = wide.shape[1:]
    tall_half = tall_in.shape[1]
    served = (gate1, up1, gate2, up2)
    down = (down1, down2)
    block = down1.shape[0]
    col = tall.shape[2]
    tokens = x.shape[0]
    side = tokens // 2
    piece = side // chips
    per_half = n_tp // 2
    lanes = chips // 2
    far = chip // 2
    lane = lax.rem(chip, 2)

    loads = {}
    sources = (
        ("down1", down1_hbm, tall_in.at[0]), ("gain1", gain1_hbm, gain.at[0]),
        ("gate1", gate1_hbm, wide.at[0]), ("up1", up1_hbm, wide.at[1]),
        ("down2", down2_hbm, tall_in.at[1]), ("gain2", gain2_hbm, gain.at[1]),
        ("gate2", gate2_hbm, wide.at[2]), ("up2", up2_hbm, wide.at[3]), ("x", x_hbm, x),
    )
    for i, (name, src, dst) in enumerate(sources):
        loads[name] = pltpu.make_async_copy(src, dst, in_sem.at[i])
        loads[name].start()

    barrier = pltpu.get_barrier_semaphore()
    for k in range(1, n_tp):
        pl.semaphore_signal(
            barrier, inc=1, device_id={"fs": f, "tp": lax.rem(t + k, n_tp)}, device_id_type=MESH
        )
    pl.semaphore_signal(barrier, inc=1, device_id={"fs": other, "tp": t}, device_id_type=MESH)
    pl.semaphore_wait(barrier, n_tp)

    def across(ref, slot):
        return pltpu.make_async_remote_copy(
            src_ref=ref, dst_ref=ref, send_sem=x_send.at[slot], recv_sem=x_recv.at[slot],
            device_id={"fs": other, "tp": t}, device_id_type=MESH,
        )

    near = rows_of(f * depth, depth, depth)

    def fold_wide(i, gain_slot):
        def one(k, _):
            rows = rows_of(k * 32, 32, 32)
            served[i][rows, near] = (gain[gain_slot] * wide[i, rows, :]).astype(BF16)
            return 0

        lax.fori_loop(0, width // 32, one, 0)
        return across(served[i].at[:, near], i)

    def fold_tall(layer):
        step = tall_half // 8

        def one(k, _):
            tall[layer, rows_of(f * tall_half + k * step, step, 16), :] = tall_in[
                layer, rows_of(k * step, step, 16), :
            ].astype(BF16)
            return 0

        lax.fori_loop(0, 8, one, 0)
        return across(tall.at[layer, rows_of(f * tall_half, tall_half, 16)], 4 + layer)

    my_cols = pl.ds(pl.multiple_of(t * col, col), col)

    def block_copy(layer, b, sender):
        return pltpu.make_async_remote_copy(
            src_ref=tall.at[layer, rows_of(b * block, block, 16)],
            dst_ref=down[layer].at[:, my_cols],
            send_sem=a_send.at[layer, b], recv_sem=a_recv.at[layer, sender],
            device_id={"fs": f, "tp": b}, device_id_type=MESH,
        )

    def hand_out(layer, which):
        def one(k, _):
            b = which * per_half + lax.rem(t + k, per_half)

            @pl.when(b != t)
            def _():
                block_copy(layer, b, t).start()

            return 0

        lax.fori_loop(0, per_half, one, 0)

    def collect(layer):
        def one(k, _):
            block_copy(layer, t, lax.rem(t + k, n_tp)).wait_recv()
            return 0

        lax.fori_loop(1, n_tp, one, 0)
        down[layer][:, my_cols] = tall[layer, rows_of(t * block, block, 16), :]

    sends = []
    loads["down1"].wait()
    tall_one = fold_tall(0)
    tall_one.start()
    hand_out(0, f)
    loads["down2"].wait()
    tall_two = fold_tall(1)
    tall_two.start()
    hand_out(1, f)
    loads["gain1"].wait()
    loads["gate1"].wait()
    gate_one = fold_wide(0, 0)
    loads["up1"].wait()
    up_one = fold_wide(1, 0)
    loads["gain2"].wait()
    loads["gate2"].wait()
    gate_two = fold_wide(2, 1)
    loads["up2"].wait()
    up_two = fold_wide(3, 1)
    loads["x"].wait()

    def unit(v):
        return (v * lax.rsqrt(jnp.mean(v * v, axis=-1, keepdims=True) + EPS)).astype(BF16)

    def norm(k, _):
        rows = rows_of(k * 32, 32, 32)
        normed[0, rows, :] = unit(x[rows, :].astype(F32))
        return 0

    lax.fori_loop(0, tokens // 32, norm, 0)
    tall_one.wait_recv()
    gate_one.start()
    hand_out(0, other)
    tall_two.wait_recv()
    up_one.start()
    hand_out(1, other)

    turned = (((1,), (1,)), ((), ()))

    def hide(layer):
        gate, up = served[2 * layer], served[2 * layer + 1]
        step = tokens // 2

        def one(k, _):
            rows = rows_of(k * step, step, step)
            v = normed[layer, rows, :]
            g = lax.dot_general(v, gate[...], turned, preferred_element_type=F32)
            u = lax.dot_general(v, up[...], turned, preferred_element_type=F32)
            hidden[rows, :] = (g / (1.0 + jnp.exp(-g)) * u).astype(BF16)
            return 0

        lax.fori_loop(0, 2, one, 0)

    def spot(z, y):
        return (y * lanes + z) * piece

    def rows_at(c, z, y):
        return rows_of(c * side + spot(z, y), piece, piece)

    def to(tp, src, dst, send, recv):
        return pltpu.make_async_remote_copy(
            src_ref=src, dst_ref=dst, send_sem=send, recv_sem=recv,
            device_id={"fs": f, "tp": tp}, device_id_type=MESH,
        )

    beside = 2 * (2 * far + 1 - lane) + core

    def at_far(z):
        return 2 * (2 * z + lane) + core

    def swap(layer, y):
        half = side // 2
        src = part.at[layer, rows_of((1 - core) * side + y * half, half, half)]
        return to(sibling, src, pair.at[layer, rows_of(y * half, half, half)],
                  p_send.at[layer, y], p_recv.at[layer, y])

    def y_copy(layer, z):
        return to(beside, ysend.at[layer, z], yrecv.at[layer, z], y_send.at[layer, z], y_recv.at[layer, z])

    def z_copy(layer, z, sender):
        return to(at_far(z), zsend.at[layer, z], zrecv.at[layer, sender],
                  s_send.at[layer, z], s_recv.at[layer, sender])

    own = rows_at(core, far, lane)

    def project(layer):
        def rows_for(c):
            rows = rows_of(c * side, side, side)
            p = jnp.dot(hidden[rows, :], down[layer][...], preferred_element_type=F32)
            part[layer, rows, :] = p.astype(BF16)

        rows_for(1 - core)
        swap(layer, 1 - lane).start()
        swap(layer, lane).start()
        rows_for(core)

    def two(layer, z, y):
        return part[layer, rows_at(core, z, y), :].astype(F32) + pair[
            layer, rows_of(spot(z, y), piece, piece), :
        ].astype(F32)

    def reduce(layer):
        swap(layer, 1 - lane).wait_recv()

        def step_y(k, _):
            z = lax.rem(far + k, lanes)
            ysend[layer, z] = two(layer, z, 1 - lane).astype(BF16)
            y_copy(layer, z).start()
            return 0

        lax.fori_loop(1, lanes + 1, step_y, 0)
        swap(layer, lane).wait_recv()

        def step_z(k, _):
            z = lax.rem(far + k, lanes)
            y_copy(layer, z).wait_recv()
            zsend[layer, z] = (two(layer, z, lane) + yrecv[layer, z].astype(F32)).astype(BF16)
            z_copy(layer, z, far).start()
            return 0

        lax.fori_loop(1, lanes, step_z, 0)
        y_copy(layer, far).wait_recv()
        total = two(layer, far, lane) + yrecv[layer, far].astype(F32)
        for k in range(1, lanes):
            z = lax.rem(far + lanes - k, lanes)
            z_copy(layer, far, z).wait_recv()
            total = total + zrecv[layer, z].astype(F32)
        return total

    def gathered(layer):
        return mixed if layer else normed.at[1]

    def piece_copy(layer, z, y, device, send):
        ref = gathered(layer).at[rows_at(core, z, y)]
        return to(device, ref, ref, send, g_recv.at[layer, 2 * z + y])

    def z_piece(layer, z, owner):
        return piece_copy(layer, owner, lane, at_far(z), g_send.at[layer, z])

    def y_piece(layer, z, y):
        return piece_copy(layer, z, y, beside, b_send.at[layer, z])

    def core_piece(layer, z, y, c):
        ref = gathered(layer).at[rows_at(c, z, y)]
        return to(sibling, ref, ref, h_send.at[layer, 2 * z + y], h_recv.at[layer, 2 * z + y])

    def gather(layer):
        def send_z(k, _):
            z_piece(layer, lax.rem(far + k, lanes), far).start()
            return 0

        lax.fori_loop(1, lanes, send_z, 0)
        y_piece(layer, far, lane).start()
        core_piece(layer, far, lane, core).start()

        def pass_z(k, _):
            z = lax.rem(far + lanes - k, lanes)
            z_piece(layer, far, z).wait_recv()
            y_piece(layer, z, lane).start()
            core_piece(layer, z, lane, core).start()
            return 0

        lax.fori_loop(1, lanes, pass_z, 0)

        def pass_y(k, _):
            z = lax.rem(far + lanes - k, lanes)
            y_piece(layer, z, 1 - lane).wait_recv()
            core_piece(layer, z, 1 - lane, core).start()
            return 0

        lax.fori_loop(0, lanes, pass_y, 0)

        def land(k, _):
            core_piece(layer, k // 2, lax.rem(k, 2), 1 - core).wait_recv()
            return 0

        lax.fori_loop(0, chips, land, 0)

    gate_one.wait_recv()
    gate_two.start()
    up_one.wait_recv()
    up_two.start()
    hide(0)
    collect(0)
    project(0)
    total = reduce(0)
    value = (x[own, :].astype(F32) + 0.5 * total).astype(BF16)
    middle[...] = value
    normed[1, own, :] = unit(value.astype(F32))
    gather(0)
    gate_two.wait_recv()
    up_two.wait_recv()
    hide(1)
    collect(1)
    project(1)
    total = reduce(1)
    mixed[own, :] = (middle[...].astype(F32) + 0.5 * total).astype(BF16)
    gather(1)

    for sent in (tall_one, gate_one, up_one, tall_two, gate_two, up_two):
        sent.wait_send()
    for layer in range(2):

        def drain(k, _):
            block_copy(layer, lax.rem(t + k, n_tp), t).wait_send()
            return 0

        lax.fori_loop(1, n_tp, drain, 0)
        swap(layer, 0).wait_send()
        swap(layer, 1).wait_send()

        def drain_z(k, _):
            z = lax.rem(far + k, lanes)
            z_copy(layer, z, far).wait_send()
            z_piece(layer, z, far).wait_send()
            return 0

        lax.fori_loop(1, lanes, drain_z, 0)

        def drain_y(z, _):
            y_copy(layer, z).wait_send()
            y_piece(layer, z, lane).wait_send()
            return 0

        lax.fori_loop(0, lanes, drain_y, 0)

        def drain_c(k, _):
            core_piece(layer, k // 2, lax.rem(k, 2), core).wait_send()
            return 0

        lax.fori_loop(0, chips, drain_c, 0)


def flush(*refs):
    n = len(refs) // 2
    copies = [
        pltpu.make_async_copy(src, dst, refs[-1].at[i])
        for i, (src, dst) in enumerate(zip(refs[:n], refs[n : 2 * n]))
    ]
    for copy in copies:
        copy.start()
    for copy in copies:
        copy.wait()


def fused(n_tp, x, gain1, gate1, up1, down1, gain2, gate2, up2, down2):
    depth, width = gate1.shape
    tall_half, col = down1.shape
    tokens, model = x.shape
    block = 2 * tall_half // n_tp
    chips = n_tp // 2
    lanes = chips // 2
    side = tokens // 2
    piece = side // chips
    dma = pltpu.SemaphoreType.DMA
    vmem = pltpu.VMEM
    anywhere = pl.BlockSpec(memory_space=pl.ANY)
    wide_out = vmem((width, 2 * depth), BF16)
    down_out = vmem((block, model), BF16)
    held = pl.pallas_call(
        functools.partial(kernel, n_tp),
        out_shape=(vmem(x.shape, BF16), wide_out, wide_out, down_out, wide_out, wide_out, down_out),
        in_specs=[anywhere] * 9,
        out_specs=[pl.BlockSpec(memory_space=pltpu.VMEM)] * 7,
        scratch_shapes=[
            vmem((tokens, model), BF16),
            vmem((2, 1, depth), F32),
            vmem((4, width, depth), F32),
            vmem((2, tall_half, col), F32),
            vmem((2, 2 * tall_half, col), BF16),
            vmem((2, tokens, model), BF16),
            vmem((tokens, width), BF16),
            vmem((2, tokens, model), BF16),
            vmem((2, side, model), BF16),
            vmem((2, lanes, piece, model), BF16),
            vmem((2, lanes, piece, model), BF16),
            vmem((2, lanes, piece, model), BF16),
            vmem((2, lanes, piece, model), BF16),
            vmem((piece, model), BF16),
            dma((9,)), dma((6,)), dma((6,)), dma((2, n_tp)), dma((2, n_tp)),
            dma((2, 2)), dma((2, 2)), dma((2, lanes)), dma((2, lanes)), dma((2, lanes)), dma((2, lanes)),
            dma((2, lanes)), dma((2, chips)), dma((2, lanes)), dma((2, chips)), dma((2, chips)),
        ],
        compiler_params=pltpu.CompilerParams(
            collective_id=0, has_side_effects=True, vmem_limit_bytes=54 * 1024 * 1024
        ),
        name="hand_over",
    )(x, gain1[None, :], gate1.T, up1.T, down1, gain2[None, :], gate2.T, up2.T, down2)
    mixed, gate_one, up_one, down_one, gate_two, up_two, down_two = pl.pallas_call(
        flush,
        out_shape=tuple(jax.ShapeDtypeStruct(v.shape, v.dtype) for v in held),
        in_specs=[anywhere] * 7,
        out_specs=[anywhere] * 7,
        scratch_shapes=[dma((7,))],
        compiler_params=pltpu.CompilerParams(vmem_limit_bytes=1024 * 1024),
        name="flush",
    )(*held)
    return (mixed, gate_one.T, up_one.T, down_one, gate_two.T, up_two.T, down_two)


def solution(mesh):
    placed = (
        P(("grp", "fs"), None),
        P("fs"),
        P("fs", "tp"),
        P("fs", "tp"),
        P("fs", "tp"),
        P("fs"),
        P("fs", "tp"),
        P("fs", "tp"),
        P("fs", "tp"),
    )
    paired = mesh.shape["fs"] == 2 and mesh.shape["tp"] % 4 == 0
    return jax.shard_map(
        functools.partial(fused, mesh.shape["tp"]) if paired else body,
        mesh=mesh,
        in_specs=placed,
        out_specs=(
            P(("grp", "fs"), None),
            P("grp", "tp"),
            P("grp", "tp"),
            P(("grp", "tp"), None),
            P("grp", "tp"),
            P("grp", "tp"),
            P(("grp", "tp"), None),
        ),
        check_vma=False,
    )
```

time: 161 us -> 139 us (0.86)
  local copies, waits for them, and re-layouts: 12.9 us -> 0 us
  Pallas kernels: 145 us -> 137 us
    unnamed x19 -> x0, local copies, waits for them, and re-layouts: 12.9 us -> none
    pallas_call x1 -> x2, Pallas kernels: 145 us -> 137 us  [the longest x1 134 us: fused(): pl.pallas_call(functools.partial(kernel, n_tp), out_shape=(vmem(x.shape,...]
where the time goes in v1:
time: 139 us; the launch traced here: 138 us
  Pallas kernels  137 us (99%)
    pallas_call x1, Pallas kernels, fused(): pl.pallas_call(functools.partial(kernel, n_tp), out_shape=(vmem(x.shape,...  134 us
    pallas_call x1, Pallas kernels, fused(): pl.pallas_call(flush, out_shape=tuple((jax.ShapeDtypeStruct(v.shape, v.dt...  3.8 us

profile of v1, /device:TPU:0, one launch (start us, length us, event | category | flops | bytes accessed | tf_op | source)
XLA Modules:
  0.0 138.1 jit_solution(352198605008956243)
XLA Ops:
  0.6 133.7 %hand_over.1 = (bf16[256,2048]{1,0:T(8,128)(2,1)S(1)}, bf16[352,2048]{1,0:T(8,128)(2,1)S(1)}, bf16[352,2048]{1,0:T(8,128)(2,1)S(1)}, bf16[352,2048]{1,0:T(8,128)...) custom-call(bf16[256,2048]{1,0:T(8,128)(2,1)} %x_hbm.1, ...), custom_call_target="tpu_custom_call" | custom-call | tf_op jit(solution)/shard_map/hand_over/pallas_call | solution.py:432
  134.3 3.8 %flush.1 = (bf16[256,2048]{1,0:T(8,128)(2,1)}, bf16[352,2048]{1,0:T(8,128)(2,1)}, bf16[352,2048]{1,0:T(8,128)(2,1)}, bf16[352,2048]{1,0:T(8,128)(2,1)}, bf16[352...) custom-call(bf16[256,2048]{1,0:T(8,128)(2,1)S(1)} %get-tuple-element.21.refs_0_, ...), custom_call_target="tpu_custom_call" | custom-call | tf_op jit(solution)/shard_map/flush/pallas_call | solution.py:461

commit v2 on v1

--- a/solution.py
+++ b/solution.py
@@ -67,8 +67,9 @@
     n_tp,
     x_hbm, gain1_hbm, gate1_hbm, up1_hbm, down1_hbm, gain2_hbm, gate2_hbm, up2_hbm, down2_hbm,
     mixed, gate1, up1, down1, gate2, up2, down2,
-    x, gain, wide, tall_in, tall, normed, hidden, part, pair, ysend, yrecv, zsend, zrecv, middle,
-    in_sem, x_send, x_recv, a_send, a_recv, p_send, p_recv, y_send, y_recv, s_send, s_recv,
+    x, gain, wide, tall_in, tall, normed, guest, psend, precv, kept, hidden, part, pair,
+    ysend, yrecv, zsend, zrecv, middle,
+    in_sem, x_send, x_recv, d_send, d_recv, v_send, v_recv, a_send, a_recv, p_send, p_recv, y_send, y_recv, s_send, s_recv,
     g_send, g_recv, b_send, h_send, h_recv,
 ):
     f = lax.axis_index("fs")
@@ -94,10 +95,10 @@
 
     loads = {}
     sources = (
-        ("down1", down1_hbm, tall_in.at[0]), ("gain1", gain1_hbm, gain.at[0]),
+        ("x", x_hbm, x), ("down1", down1_hbm, tall_in.at[0]), ("gain1", gain1_hbm, gain.at[0]),
         ("gate1", gate1_hbm, wide.at[0]), ("up1", up1_hbm, wide.at[1]),
         ("down2", down2_hbm, tall_in.at[1]), ("gain2", gain2_hbm, gain.at[1]),
-        ("gate2", gate2_hbm, wide.at[2]), ("up2", up2_hbm, wide.at[3]), ("x", x_hbm, x),
+        ("gate2", gate2_hbm, wide.at[2]), ("up2", up2_hbm, wide.at[3]),
     )
     for i, (name, src, dst) in enumerate(sources):
         loads[name] = pltpu.make_async_copy(src, dst, in_sem.at[i])
@@ -109,88 +110,6 @@
             barrier, inc=1, device_id={"fs": f, "tp": lax.rem(t + k, n_tp)}, device_id_type=MESH
         )
     pl.semaphore_signal(barrier, inc=1, device_id={"fs": other, "tp": t}, device_id_type=MESH)
-    pl.semaphore_wait(barrier, n_tp)
-
-    def across(ref, slot):
-        return pltpu.make_async_remote_copy(
-            src_ref=ref, dst_ref=ref, send_sem=x_send.at[slot], recv_sem=x_recv.at[slot],
-            device_id={"fs": other, "tp": t}, device_id_type=MESH,
-        )
-
-    near = rows_of(f * depth, depth, depth)
-
-    def fold_wide(i, gain_slot):
-        def one(k, _):
-            rows = rows_of(k * 32, 32, 32)
-            served[i][rows, near] = (gain[gain_slot] * wide[i, rows, :]).astype(BF16)
-            return 0
-
-        lax.fori_loop(0, width // 32, one, 0)
-        return across(served[i].at[:, near], i)
-
-    def fold_tall(layer):
-        step = tall_half // 8
-
-        def one(k, _):
-            tall[layer, rows_of(f * tall_half + k * step, step, 16), :] = tall_in[
-                layer, rows_of(k * step, step, 16), :
-            ].astype(BF16)
-            return 0
-
-        lax.fori_loop(0, 8, one, 0)
-        return across(tall.at[layer, rows_of(f * tall_half, tall_half, 16)], 4 + layer)
-
-    my_cols = pl.ds(pl.multiple_of(t * col, col), col)
-
-    def block_copy(layer, b, sender):
-        return pltpu.make_async_remote_copy(
-            src_ref=tall.at[layer, rows_of(b * block, block, 16)],
-            dst_ref=down[layer].at[:, my_cols],
-            send_sem=a_send.at[layer, b], recv_sem=a_recv.at[layer, sender],
-            device_id={"fs": f, "tp": b}, device_id_type=MESH,
-        )
-
-    def hand_out(layer, which):
-        def one(k, _):
-            b = which * per_half + lax.rem(t + k, per_half)
-
-            @pl.when(b != t)
-            def _():
-                block_copy(layer, b, t).start()
-
-            return 0
-
-        lax.fori_loop(0, per_half, one, 0)
-
-    def collect(layer):
-        def one(k, _):
-            block_copy(layer, t, lax.rem(t + k, n_tp)).wait_recv()
-            return 0
-
-        lax.fori_loop(1, n_tp, one, 0)
-        down[layer][:, my_cols] = tall[layer, rows_of(t * block, block, 16), :]
-
-    sends = []
-    loads["down1"].wait()
-    tall_one = fold_tall(0)
-    tall_one.start()
-    hand_out(0, f)
-    loads["down2"].wait()
-    tall_two = fold_tall(1)
-    tall_two.start()
-    hand_out(1, f)
-    loads["gain1"].wait()
-    loads["gate1"].wait()
-    gate_one = fold_wide(0, 0)
-    loads["up1"].wait()
-    up_one = fold_wide(1, 0)
-    loads["gain2"].wait()
-    loads["gate2"].wait()
-    gate_two = fold_wide(2, 1)
-    loads["up2"].wait()
-    up_two = fold_wide(3, 1)
-    loads["x"].wait()
-
     def unit(v):
         return (v * lax.rsqrt(jnp.mean(v * v, axis=-1, keepdims=True) + EPS)).astype(BF16)
 
@@ -199,35 +118,17 @@
         normed[0, rows, :] = unit(x[rows, :].astype(F32))
         return 0
 
+    loads["x"].wait()
     lax.fori_loop(0, tokens // 32, norm, 0)
-    tall_one.wait_recv()
-    gate_one.start()
-    hand_out(0, other)
-    tall_two.wait_recv()
-    up_one.start()
-    hand_out(1, other)
-
-    turned = (((1,), (1,)), ((), ()))
-
-    def hide(layer):
-        gate, up = served[2 * layer], served[2 * layer + 1]
-        step = tokens // 2
-
-        def one(k, _):
-            rows = rows_of(k * step, step, step)
-            v = normed[layer, rows, :]
-            g = lax.dot_general(v, gate[...], turned, preferred_element_type=F32)
-            u = lax.dot_general(v, up[...], turned, preferred_element_type=F32)
-            hidden[rows, :] = (g / (1.0 + jnp.exp(-g)) * u).astype(BF16)
-            return 0
-
-        lax.fori_loop(0, 2, one, 0)
-
-    def spot(z, y):
-        return (y * lanes + z) * piece
-
-    def rows_at(c, z, y):
-        return rows_of(c * side + spot(z, y), piece, piece)
+
+    near = rows_of(f * depth, depth, depth)
+    away = rows_of(other * depth, depth, depth)
+
+    def across(src, dst, send, recv):
+        return pltpu.make_async_remote_copy(
+            src_ref=src, dst_ref=dst, send_sem=send, recv_sem=recv,
+            device_id={"fs": other, "tp": t}, device_id_type=MESH,
+        )
 
     def to(tp, src, dst, send, recv):
         return pltpu.make_async_remote_copy(
@@ -235,7 +136,174 @@
             device_id={"fs": f, "tp": tp}, device_id_type=MESH,
         )
 
+    def wide_copy(i):
+        ref = served[i].at[:, near]
+        return across(ref, ref, x_send.at[i], x_recv.at[i])
+
+    def fold_wide(i, gain_slot):
+        def one(k, _):
+            rows = rows_of(k * 32, 32, 32)
+            served[i][rows, near] = (gain[gain_slot] * wide[i, rows, :]).astype(BF16)
+            return 0
+
+        lax.fori_loop(0, width // 32, one, 0)
+
+    def fold_tall(layer):
+        step = tall_half // 8
+
+        def one(k, _):
+            tall[layer, rows_of(f * tall_half + k * step, step, 16), :] = tall_in[
+                layer, rows_of(k * step, step, 16), :
+            ].astype(BF16)
+            return 0
+
+        lax.fori_loop(0, 8, one, 0)
+
+    my_cols = pl.ds(pl.multiple_of(t * col, col), col)
+
+    def block_copy(layer, b, sender):
+        return to(
+            b, tall.at[layer, rows_of(b * block, block, 16)], down[layer].at[:, my_cols],
+            a_send.at[layer, b], a_recv.at[layer, sender],
+        )
+
+    def tall_copy(layer, b):
+        ref = tall.at[layer, rows_of(b * block, block, 16)]
+        return across(ref, ref, d_send.at[layer, b], d_recv.at[layer, b])
+
+    def turn(which, k):
+        return which * per_half + lax.rem(t + k, per_half)
+
+    def cross_tall(layer):
+        def one(k, _):
+            tall_copy(layer, turn(f, k)).start()
+            return 0
+
+        lax.fori_loop(0, per_half, one, 0)
+
+    def hand_out(layer, first, last):
+        def one(k, _):
+            b = turn(f, k)
+
+            @pl.when(b != t)
+            def _():
+                block_copy(layer, b, t).start()
+
+            return 0
+
+        lax.fori_loop(first, last, one, 0)
+
+    def pass_on(layer, first, last):
+        def one(k, _):
+            b = turn(other, k)
+            tall_copy(layer, b).wait_recv()
+
+            @pl.when(b != t)
+            def _():
+                block_copy(layer, b, t).start()
+
+            return 0
+
+        lax.fori_loop(first, last, one, 0)
+
+    def collect(layer):
+        def one(k, _):
+            block_copy(layer, t, lax.rem(t + k, n_tp)).wait_recv()
+            return 0
+
+        lax.fori_loop(1, n_tp, one, 0)
+        down[layer][:, my_cols] = tall[layer, rows_of(t * block, block, 16), :]
+
     beside = 2 * (2 * far + 1 - lane) + core
+    quarter = tokens // 4
+
+    def share(y, c):
+        return rows_of((2 * y + c) * quarter, quarter, quarter)
+
+    guest_in = across(
+        normed.at[0, share(lane, core), away], guest.at[share(lane, core)], v_send.at[0], v_recv.at[0]
+    )
+
+    def guest_copy(device, y, c, slot):
+        ref = guest.at[share(y, c)]
+        return to(device, ref, ref, v_send.at[slot], v_recv.at[slot])
+
+    loads["down1"].wait()
+    fold_tall(0)
+    pl.semaphore_wait(barrier, n_tp)
+    guest_in.start()
+    cross_tall(0)
+    hand_out(0, 0, per_half)
+    loads["gain1"].wait()
+    loads["gate1"].wait()
+    fold_wide(0, 0)
+    loads["up1"].wait()
+    fold_wide(1, 0)
+    guest_in.wait_recv()
+    guest_copy(beside, lane, core, 1).start()
+    guest_copy(sibling, lane, core, 2).start()
+    loads["down2"].wait()
+    fold_tall(1)
+    pass_on(0, 0, 1)
+    guest_copy(beside, 1 - lane, core, 1).wait_recv()
+    guest_copy(sibling, 1 - lane, core, 3).start()
+    loads["gain2"].wait()
+    loads["gate2"].wait()
+    fold_wide(2, 1)
+    loads["up2"].wait()
+    fold_wide(3, 1)
+    guest_copy(sibling, lane, 1 - core, 2).wait_recv()
+    guest_copy(sibling, 1 - lane, 1 - core, 3).wait_recv()
+
+    turned = (((1,), (1,)), ((), ()))
+
+    def times(rows, i, cols):
+        return lax.dot_general(rows, served[i][:, cols], turned, preferred_element_type=F32)
+
+    def partial_copy(i):
+        return across(psend.at[i], precv.at[i], v_send.at[4 + i], v_recv.at[4 + i])
+
+    for i in range(2):
+        psend[i] = times(guest[...], i, near).astype(BF16)
+        partial_copy(i).start()
+    cross_tall(1)
+    for i in (2, 3, 0, 1):
+        wide_copy(i).start()
+    pass_on(0, 1, 3)
+    for i in range(2):
+        kept[i] = times(normed[0, :, near], i, near)
+    pass_on(0, 3, per_half)
+
+    def gated(rows, g, u):
+        hidden[rows, :] = (g / (1.0 + jnp.exp(-g)) * u).astype(BF16)
+
+    def hide_one():
+        def one(k, _):
+            rows = rows_of(k * 32, 32, 32)
+            gated(rows, kept[0, rows, :] + precv[0, rows, :].astype(F32),
+                  kept[1, rows, :] + precv[1, rows, :].astype(F32))
+            return 0
+
+        lax.fori_loop(0, tokens // 32, one, 0)
+
+    def hide_two():
+        step = tokens // 2
+
+        def one(k, _):
+            rows = rows_of(k * step, step, step)
+            v = normed[1, rows, :]
+            g = lax.dot_general(v, gate2[...], turned, preferred_element_type=F32)
+            u = lax.dot_general(v, up2[...], turned, preferred_element_type=F32)
+            gated(rows, g, u)
+            return 0
+
+        lax.fori_loop(0, 2, one, 0)
+
+    def spot(z, y):
+        return (y * lanes + z) * piece
+
+    def rows_at(c, z, y):
+        return rows_of(c * side + spot(z, y), piece, piece)
 
     def at_far(z):
         return 2 * (2 * z + lane) + core
@@ -271,7 +339,7 @@
             layer, rows_of(spot(z, y), piece, piece), :
         ].astype(F32)
 
-    def reduce(layer):
+    def reduce(layer, then):
         swap(layer, 1 - lane).wait_recv()
 
         def step_y(k, _):
@@ -291,6 +359,7 @@
             return 0
 
         lax.fori_loop(1, lanes, step_z, 0)
+        then()
         y_copy(layer, far).wait_recv()
         total = two(layer, far, lane) + yrecv[layer, far].astype(F32)
         for k in range(1, lanes):
@@ -316,12 +385,13 @@
         ref = gathered(layer).at[rows_at(c, z, y)]
         return to(sibling, ref, ref, h_send.at[layer, 2 * z + y], h_recv.at[layer, 2 * z + y])
 
-    def gather(layer):
+    def gather(layer, then):
         def send_z(k, _):
             z_piece(layer, lax.rem(far + k, lanes), far).start()
             return 0
 
         lax.fori_loop(1, lanes, send_z, 0)
+        then()
         y_piece(layer, far, lane).start()
         core_piece(layer, far, lane, core).start()
 
@@ -348,29 +418,46 @@
 
         lax.fori_loop(0, chips, land, 0)
 
-    gate_one.wait_recv()
-    gate_two.start()
-    up_one.wait_recv()
-    up_two.start()
-    hide(0)
+    def more(own_from, own_to, first, last):
+        def act():
+            hand_out(1, own_from, own_to)
+            pass_on(1, first, last)
+
+        return act
+
+    def rest():
+        return None
+
+    for i in range(2):
+        partial_copy(i).wait_recv()
+    hide_one()
+    hand_out(1, 0, 2)
     collect(0)
     project(0)
-    total = reduce(0)
+    total = reduce(0, more(2, 5, 0, 3))
     value = (x[own, :].astype(F32) + 0.5 * total).astype(BF16)
     middle[...] = value
     normed[1, own, :] = unit(value.astype(F32))
-    gather(0)
-    gate_two.wait_recv()
-    up_two.wait_recv()
-    hide(1)
+    gather(0, more(5, per_half, 3, per_half))
+    wide_copy(2).wait_recv()
+    wide_copy(3).wait_recv()
+    hide_two()
     collect(1)
     project(1)
-    total = reduce(1)
+    total = reduce(1, rest)
     mixed[own, :] = (middle[...].astype(F32) + 0.5 * total).astype(BF16)
-    gather(1)
-
-    for sent in (tall_one, gate_one, up_one, tall_two, gate_two, up_two):
-        sent.wait_send()
+    gather(1, rest)
+
+    wide_copy(0).wait_recv()
+    wide_copy(1).wait_recv()
+    for i in range(4):
+        wide_copy(i).wait_send()
+    for i in range(2):
+        partial_copy(i).wait_send()
+    guest_in.wait_send()
+    guest_copy(beside, lane, core, 1).wait_send()
+    guest_copy(sibling, lane, core, 2).wait_send()
+    guest_copy(sibling, 1 - lane, core, 3).wait_send()
     for layer in range(2):
 
         def drain(k, _):
@@ -378,6 +465,12 @@
             return 0
 
         lax.fori_loop(1, n_tp, drain, 0)
+
+        def drain_x(k, _):
+            tall_copy(layer, turn(f, k)).wait_send()
+            return 0
+
+        lax.fori_loop(0, per_half, drain_x, 0)
         swap(layer, 0).wait_send()
         swap(layer, 1).wait_send()
 
@@ -441,6 +534,10 @@
             vmem((2, tall_half, col), F32),
             vmem((2, 2 * tall_half, col), BF16),
             vmem((2, tokens, model), BF16),
+            vmem((tokens, depth), BF16),
+            vmem((2, tokens, width), BF16),
+            vmem((2, tokens, width), BF16),
+            vmem((2, tokens, width), F32),
             vmem((tokens, width), BF16),
             vmem((2, tokens, model), BF16),
             vmem((2, side, model), BF16),
@@ -449,7 +546,8 @@
             vmem((2, lanes, piece, model), BF16),
             vmem((2, lanes, piece, model), BF16),
             vmem((piece, model), BF16),
-            dma((9,)), dma((6,)), dma((6,)), dma((2, n_tp)), dma((2, n_tp)),
+            dma((9,)), dma((4,)), dma((4,)), dma((2, n_tp)), dma((2, n_tp)), dma((6,)), dma((6,)),
+            dma((2, n_tp)), dma((2, n_tp)),
             dma((2, 2)), dma((2, 2)), dma((2, lanes)), dma((2, lanes)), dma((2, lanes)), dma((2, lanes)),
             dma((2, lanes)), dma((2, chips)), dma((2, lanes)), dma((2, chips)), dma((2, chips)),
         ],

time: 139 us -> 125 us (0.90)
  the two profiles are of different devices: /device:TPU:0 before, /device:TPU:21 now
where the time goes in v2:
time: 125 us
  Pallas kernels  124 us (99%)
    pallas_call x1, Pallas kernels, fused(): pl.pallas_call(functools.partial(kernel, n_tp), out_shape=(vmem(x.shape,...  120 us
    pallas_call x1, Pallas kernels, fused(): pl.pallas_call(flush, out_shape=tuple((jax.ShapeDtypeStruct(v.shape, v.dt...  3.8 us

profile of v2, /device:TPU:21, one launch (start us, length us, event | category | flops | bytes accessed | tf_op | source)
XLA Modules:
  0.0 124.7 jit_solution(12102853633222097889)
XLA Ops:
  0.6 120.2 %hand_over.1 = (bf16[256,2048]{1,0:T(8,128)(2,1)S(1)}, bf16[352,2048]{1,0:T(8,128)(2,1)S(1)}, bf16[352,2048]{1,0:T(8,128)(2,1)S(1)}, bf16[352,2048]{1,0:T(8,128)...) custom-call(bf16[256,2048]{1,0:T(8,128)(2,1)} %x_hbm.1, ...), custom_call_target="tpu_custom_call" | custom-call | tf_op jit(solution)/shard_map/hand_over/pallas_call | solution.py:525
  120.8 3.8 %flush.1 = (bf16[256,2048]{1,0:T(8,128)(2,1)}, bf16[352,2048]{1,0:T(8,128)(2,1)}, bf16[352,2048]{1,0:T(8,128)(2,1)}, bf16[352,2048]{1,0:T(8,128)(2,1)}, bf16[352...) custom-call(bf16[256,2048]{1,0:T(8,128)(2,1)S(1)} %get-tuple-element.21.refs_0_, ...), custom_call_target="tpu_custom_call" | custom-call | tf_op jit(solution)/shard_map/flush/pallas_call | solution.py:559

commit v3 on v2

--- a/solution.py
+++ b/solution.py
@@ -89,6 +89,9 @@
     side = tokens // 2
     piece = side // chips
     per_half = n_tp // 2
+    eighth = per_half // 8
+    own_cuts = (2 * eighth, 5 * eighth, per_half)
+    cross_cuts = (0, 3 * eighth, per_half)
     lanes = chips // 2
     far = chip // 2
     lane = lax.rem(chip, 2)
@@ -172,14 +175,16 @@
         return across(ref, ref, d_send.at[layer, b], d_recv.at[layer, b])
 
     def turn(which, k):
-        return which * per_half + lax.rem(t + k, per_half)
-
-    def cross_tall(layer):
+        y = lax.rem(lane + k // lanes, 2)
+        z = lax.rem(far + k // 2, lanes // 2)
+        return which * per_half + (2 * z + y) * 2 + lax.rem(core + k, 2)
+
+    def cross_tall(layer, first, last):
         def one(k, _):
             tall_copy(layer, turn(f, k)).start()
             return 0
 
-        lax.fori_loop(0, per_half, one, 0)
+        lax.fori_loop(first, last, one, 0)
 
     def hand_out(layer, first, last):
         def one(k, _):
@@ -231,29 +236,33 @@
     loads["down1"].wait()
     fold_tall(0)
     pl.semaphore_wait(barrier, n_tp)
+    cross_tall(0, 0, eighth)
     guest_in.start()
-    cross_tall(0)
-    hand_out(0, 0, per_half)
+    cross_tall(0, eighth, per_half)
+    hand_out(0, 0, 4 * eighth)
     loads["gain1"].wait()
     loads["gate1"].wait()
     fold_wide(0, 0)
     loads["up1"].wait()
     fold_wide(1, 0)
+    pass_on(0, 0, eighth)
     guest_in.wait_recv()
     guest_copy(beside, lane, core, 1).start()
     guest_copy(sibling, lane, core, 2).start()
     loads["down2"].wait()
     fold_tall(1)
-    pass_on(0, 0, 1)
-    guest_copy(beside, 1 - lane, core, 1).wait_recv()
-    guest_copy(sibling, 1 - lane, core, 3).start()
     loads["gain2"].wait()
     loads["gate2"].wait()
     fold_wide(2, 1)
     loads["up2"].wait()
     fold_wide(3, 1)
+    pass_on(0, eighth, 3 * eighth)
+    guest_copy(beside, 1 - lane, core, 1).wait_recv()
+    guest_copy(sibling, 1 - lane, core, 3).start()
+    pass_on(0, 3 * eighth, 4 * eighth)
     guest_copy(sibling, lane, 1 - core, 2).wait_recv()
     guest_copy(sibling, 1 - lane, 1 - core, 3).wait_recv()
+    hand_out(0, 4 * eighth, per_half)
 
     turned = (((1,), (1,)), ((), ()))
 
@@ -266,13 +275,13 @@
     for i in range(2):
         psend[i] = times(guest[...], i, near).astype(BF16)
         partial_copy(i).start()
-    cross_tall(1)
+    cross_tall(1, 0, per_half)
     for i in (2, 3, 0, 1):
         wide_copy(i).start()
-    pass_on(0, 1, 3)
+    pass_on(0, 4 * eighth, 6 * eighth)
     for i in range(2):
         kept[i] = times(normed[0, :, near], i, near)
-    pass_on(0, 3, per_half)
+    pass_on(0, 6 * eighth, per_half)
 
     def gated(rows, g, u):
         hidden[rows, :] = (g / (1.0 + jnp.exp(-g)) * u).astype(BF16)
@@ -287,17 +296,12 @@
         lax.fori_loop(0, tokens // 32, one, 0)
 
     def hide_two():
-        step = tokens // 2
-
-        def one(k, _):
-            rows = rows_of(k * step, step, step)
-            v = normed[1, rows, :]
-            g = lax.dot_general(v, gate2[...], turned, preferred_element_type=F32)
-            u = lax.dot_general(v, up2[...], turned, preferred_element_type=F32)
-            gated(rows, g, u)
-            return 0
-
-        lax.fori_loop(0, 2, one, 0)
+        gated(slice(None), times(normed[1], 2, slice(None)), times(normed[1], 3, slice(None)))
+
+    def peer(k):
+        m = k + lanes // 2 - 1
+        m = jnp.where(m < lanes, m, jnp.where(k == lanes, 0, m - lanes + 1))
+        return lax.bitwise_xor(far, m)
 
     def spot(z, y):
         return (y * lanes + z) * piece
@@ -343,7 +347,7 @@
         swap(layer, 1 - lane).wait_recv()
 
         def step_y(k, _):
-            z = lax.rem(far + k, lanes)
+            z = peer(k)
             ysend[layer, z] = two(layer, z, 1 - lane).astype(BF16)
             y_copy(layer, z).start()
             return 0
@@ -352,18 +356,18 @@
         swap(layer, lane).wait_recv()
 
         def step_z(k, _):
-            z = lax.rem(far + k, lanes)
+            z = peer(k)
             y_copy(layer, z).wait_recv()
             zsend[layer, z] = (two(layer, z, lane) + yrecv[layer, z].astype(F32)).astype(BF16)
             z_copy(layer, z, far).start()
             return 0
 
         lax.fori_loop(1, lanes, step_z, 0)
-        then()
+        then(0)
         y_copy(layer, far).wait_recv()
         total = two(layer, far, lane) + yrecv[layer, far].astype(F32)
         for k in range(1, lanes):
-            z = lax.rem(far + lanes - k, lanes)
+            z = peer(k)
             z_copy(layer, far, z).wait_recv()
             total = total + zrecv[layer, z].astype(F32)
         return total
@@ -387,27 +391,29 @@
 
     def gather(layer, then):
         def send_z(k, _):
-            z_piece(layer, lax.rem(far + k, lanes), far).start()
+            z_piece(layer, peer(k), far).start()
             return 0
 
         lax.fori_loop(1, lanes, send_z, 0)
-        then()
+        then(1)
         y_piece(layer, far, lane).start()
         core_piece(layer, far, lane, core).start()
 
         def pass_z(k, _):
-            z = lax.rem(far + lanes - k, lanes)
+            z = peer(k)
             z_piece(layer, far, z).wait_recv()
             y_piece(layer, z, lane).start()
             core_piece(layer, z, lane, core).start()
+            then(1 + k)
             return 0
 
         lax.fori_loop(1, lanes, pass_z, 0)
 
         def pass_y(k, _):
-            z = lax.rem(far + lanes - k, lanes)
+            z = peer(jnp.where(k == 0, lanes, k))
             y_piece(layer, z, 1 - lane).wait_recv()
             core_piece(layer, z, 1 - lane, core).start()
+            then(1 + lanes + k)
             return 0
 
         lax.fori_loop(0, lanes, pass_y, 0)
@@ -418,27 +424,28 @@
 
         lax.fori_loop(0, chips, land, 0)
 
-    def more(own_from, own_to, first, last):
-        def act():
-            hand_out(1, own_from, own_to)
-            pass_on(1, first, last)
-
-        return act
-
-    def rest():
+    def dole(k):
+        if isinstance(k, int) and k + 1 < len(own_cuts):
+            hand_out(1, own_cuts[k], own_cuts[k + 1])
+            pass_on(1, cross_cuts[k], cross_cuts[k + 1])
+
+    def rest(k):
         return None
 
     for i in range(2):
         partial_copy(i).wait_recv()
     hide_one()
-    hand_out(1, 0, 2)
+    hand_out(1, 0, own_cuts[0])
     collect(0)
+    pass_on(1, 0, cross_cuts[0])
     project(0)
-    total = reduce(0, more(2, 5, 0, 3))
+    total = reduce(0, dole)
     value = (x[own, :].astype(F32) + 0.5 * total).astype(BF16)
     middle[...] = value
     normed[1, own, :] = unit(value.astype(F32))
-    gather(0, more(5, per_half, 3, per_half))
+    gather(0, dole)
+    hand_out(1, own_cuts[-1], per_half)
+    pass_on(1, cross_cuts[-1], per_half)
     wide_copy(2).wait_recv()
     wide_copy(3).wait_recv()
     hide_two()
@@ -580,9 +587,10 @@
         P("fs", "tp"),
         P("fs", "tp"),
     )
-    paired = mesh.shape["fs"] == 2 and mesh.shape["tp"] % 4 == 0
+    tp = mesh.shape["tp"]
+    paired = mesh.shape["fs"] == 2 and tp % 16 == 0 and tp & (tp - 1) == 0
     return jax.shard_map(
-        functools.partial(fused, mesh.shape["tp"]) if paired else body,
+        functools.partial(fused, tp) if paired else body,
         mesh=mesh,
         in_specs=placed,
         out_specs=(

time: 125 us -> 121 us (0.968)
  the two profiles are of different devices: /device:TPU:21 before, /device:TPU:0 now
where the time goes in v3:
time: 121 us; the launch traced here: 120 us
  Pallas kernels  120 us (99%)
    pallas_call x1, Pallas kernels, fused(): pl.pallas_call(functools.partial(kernel, n_tp), out_shape=(vmem(x.shape,...  116 us
    pallas_call x1, Pallas kernels, fused(): pl.pallas_call(flush, out_shape=tuple((jax.ShapeDtypeStruct(v.shape, v.dt...  3.8 us

profile of v3, /device:TPU:0, one launch (start us, length us, event | category | flops | bytes accessed | tf_op | source)
XLA Modules:
  0.0 120.4 jit_solution(16857056017214499204)
XLA Ops:
  0.6 116.0 %hand_over.1 = (bf16[256,2048]{1,0:T(8,128)(2,1)S(1)}, bf16[352,2048]{1,0:T(8,128)(2,1)S(1)}, bf16[352,2048]{1,0:T(8,128)(2,1)S(1)}, bf16[352,2048]{1,0:T(8,128)...) custom-call(bf16[256,2048]{1,0:T(8,128)(2,1)} %x_hbm.1, ...), custom_call_target="tpu_custom_call" | custom-call | tf_op jit(solution)/shard_map/hand_over/pallas_call | solution.py:532
  116.6 3.8 %flush.1 = (bf16[256,2048]{1,0:T(8,128)(2,1)}, bf16[352,2048]{1,0:T(8,128)(2,1)}, bf16[352,2048]{1,0:T(8,128)(2,1)}, bf16[352,2048]{1,0:T(8,128)(2,1)}, bf16[352...) custom-call(bf16[256,2048]{1,0:T(8,128)(2,1)S(1)} %get-tuple-element.21.refs_0_, ...), custom_call_target="tpu_custom_call" | custom-call | tf_op jit(solution)/shard_map/flush/pallas_call | solution.py:566

commit v4 on v3

--- a/solution.py
+++ b/solution.py
@@ -69,7 +69,8 @@
     mixed, gate1, up1, down1, gate2, up2, down2,
     x, gain, wide, tall_in, tall, normed, guest, psend, precv, kept, hidden, part, pair,
     ysend, yrecv, zsend, zrecv, middle,
-    in_sem, x_send, x_recv, d_send, d_recv, v_send, v_recv, a_send, a_recv, p_send, p_recv, y_send, y_recv, s_send, s_recv,
+    in_sem, x_send, x_recv, d_send, d_recv, v_send, v_recv, a_send, a_recv, p_send, p_recv,
+    y_send, y_recv, s_send, s_recv,
     g_send, g_recv, b_send, h_send, h_recv,
 ):
     f = lax.axis_index("fs")
@@ -96,9 +97,16 @@
     far = chip // 2
     lane = lax.rem(chip, 2)
 
+    barrier = pltpu.get_barrier_semaphore()
+    for k in range(1, n_tp):
+        pl.semaphore_signal(
+            barrier, inc=1, device_id={"fs": f, "tp": lax.rem(t + k, n_tp)}, device_id_type=MESH
+        )
+    pl.semaphore_signal(barrier, inc=1, device_id={"fs": other, "tp": t}, device_id_type=MESH)
+
     loads = {}
     sources = (
-        ("x", x_hbm, x), ("down1", down1_hbm, tall_in.at[0]), ("gain1", gain1_hbm, gain.at[0]),
+        ("down1", down1_hbm, tall_in.at[0]), ("x", x_hbm, x), ("gain1", gain1_hbm, gain.at[0]),
         ("gate1", gate1_hbm, wide.at[0]), ("up1", up1_hbm, wide.at[1]),
         ("down2", down2_hbm, tall_in.at[1]), ("gain2", gain2_hbm, gain.at[1]),
         ("gate2", gate2_hbm, wide.at[2]), ("up2", up2_hbm, wide.at[3]),
@@ -107,12 +115,6 @@
         loads[name] = pltpu.make_async_copy(src, dst, in_sem.at[i])
         loads[name].start()
 
-    barrier = pltpu.get_barrier_semaphore()
-    for k in range(1, n_tp):
-        pl.semaphore_signal(
-            barrier, inc=1, device_id={"fs": f, "tp": lax.rem(t + k, n_tp)}, device_id_type=MESH
-        )
-    pl.semaphore_signal(barrier, inc=1, device_id={"fs": other, "tp": t}, device_id_type=MESH)
     def unit(v):
         return (v * lax.rsqrt(jnp.mean(v * v, axis=-1, keepdims=True) + EPS)).astype(BF16)
 
@@ -120,9 +122,6 @@
         rows = rows_of(k * 32, 32, 32)
         normed[0, rows, :] = unit(x[rows, :].astype(F32))
         return 0
-
-    loads["x"].wait()
-    lax.fori_loop(0, tokens // 32, norm, 0)
 
     near = rows_of(f * depth, depth, depth)
     away = rows_of(other * depth, depth, depth)
@@ -164,15 +163,15 @@
 
     my_cols = pl.ds(pl.multiple_of(t * col, col), col)
 
-    def block_copy(layer, b, sender):
+    def block_copy(layer, b):
         return to(
             b, tall.at[layer, rows_of(b * block, block, 16)], down[layer].at[:, my_cols],
-            a_send.at[layer, b], a_recv.at[layer, sender],
+            a_send.at[layer], a_recv.at[layer],
         )
 
     def tall_copy(layer, b):
         ref = tall.at[layer, rows_of(b * block, block, 16)]
-        return across(ref, ref, d_send.at[layer, b], d_recv.at[layer, b])
+        return across(ref, ref, d_send.at[layer], d_recv.at[layer, lax.rem(b, per_half)])
 
     def turn(which, k):
         y = lax.rem(lane + k // lanes, 2)
@@ -192,7 +191,7 @@
 
             @pl.when(b != t)
             def _():
-                block_copy(layer, b, t).start()
+                block_copy(layer, b).start()
 
             return 0
 
@@ -205,18 +204,18 @@
 
             @pl.when(b != t)
             def _():
-                block_copy(layer, b, t).start()
+                block_copy(layer, b).start()
 
             return 0
 
         lax.fori_loop(first, last, one, 0)
 
+    def all_blocks(layer):
+        ref = down[layer].at[:, pl.ds(0, (n_tp - 1) * col)]
+        return to(sibling, ref, ref, a_send.at[layer], a_recv.at[layer])
+
     def collect(layer):
-        def one(k, _):
-            block_copy(layer, t, lax.rem(t + k, n_tp)).wait_recv()
-            return 0
-
-        lax.fori_loop(1, n_tp, one, 0)
+        all_blocks(layer).wait_recv()
         down[layer][:, my_cols] = tall[layer, rows_of(t * block, block, 16), :]
 
     beside = 2 * (2 * far + 1 - lane) + core
@@ -237,9 +236,11 @@
     fold_tall(0)
     pl.semaphore_wait(barrier, n_tp)
     cross_tall(0, 0, eighth)
+    hand_out(0, 0, 4 * eighth)
+    loads["x"].wait()
+    lax.fori_loop(0, tokens // 32, norm, 0)
     guest_in.start()
     cross_tall(0, eighth, per_half)
-    hand_out(0, 0, 4 * eighth)
     loads["gain1"].wait()
     loads["gate1"].wait()
     fold_wide(0, 0)
@@ -298,10 +299,9 @@
     def hide_two():
         gated(slice(None), times(normed[1], 2, slice(None)), times(normed[1], 3, slice(None)))
 
-    def peer(k):
-        m = k + lanes // 2 - 1
-        m = jnp.where(m < lanes, m, jnp.where(k == lanes, 0, m - lanes + 1))
-        return lax.bitwise_xor(far, m)
+    near_z = lax.bitwise_xor(far, 1)
+    over_z = lax.bitwise_xor(far, 2)
+    last_z = lax.bitwise_xor(far, 3)
 
     def spot(z, y):
         return (y * lanes + z) * piece
@@ -316,14 +316,14 @@
         half = side // 2
         src = part.at[layer, rows_of((1 - core) * side + y * half, half, half)]
         return to(sibling, src, pair.at[layer, rows_of(y * half, half, half)],
-                  p_send.at[layer, y], p_recv.at[layer, y])
+                  p_send.at[layer], p_recv.at[layer, y])
 
     def y_copy(layer, z):
-        return to(beside, ysend.at[layer, z], yrecv.at[layer, z], y_send.at[layer, z], y_recv.at[layer, z])
-
-    def z_copy(layer, z, sender):
-        return to(at_far(z), zsend.at[layer, z], zrecv.at[layer, sender],
-                  s_send.at[layer, z], s_recv.at[layer, sender])
+        return to(beside, ysend.at[layer, z], yrecv.at[layer, z], y_send.at[layer], y_recv.at[layer, z])
+
+    def z_copy(layer, z, device, slot):
+        return to(at_far(device), zsend.at[layer, z], zrecv.at[layer, slot],
+                  s_send.at[layer], s_recv.at[layer, slot])
 
     own = rows_at(core, far, lane)
 
@@ -346,30 +346,27 @@
     def reduce(layer, then):
         swap(layer, 1 - lane).wait_recv()
 
-        def step_y(k, _):
-            z = peer(k)
+        for z in (last_z, near_z, over_z, far):
             ysend[layer, z] = two(layer, z, 1 - lane).astype(BF16)
             y_copy(layer, z).start()
-            return 0
-
-        lax.fori_loop(1, lanes + 1, step_y, 0)
         swap(layer, lane).wait_recv()
 
-        def step_z(k, _):
-            z = peer(k)
+        def summed(z):
             y_copy(layer, z).wait_recv()
-            zsend[layer, z] = (two(layer, z, lane) + yrecv[layer, z].astype(F32)).astype(BF16)
-            z_copy(layer, z, far).start()
-            return 0
-
-        lax.fori_loop(1, lanes, step_z, 0)
+            return two(layer, z, lane) + yrecv[layer, z].astype(F32)
+
+        for z in (last_z, near_z):
+            zsend[layer, z] = summed(z).astype(BF16)
+            z_copy(layer, z, near_z, z).start()
+        total = summed(over_z)
+        z_copy(layer, far, far, over_z).wait_recv()
+        zsend[layer, over_z] = (total + zrecv[layer, over_z].astype(F32)).astype(BF16)
+        z_copy(layer, over_z, over_z, last_z).start()
         then(0)
-        y_copy(layer, far).wait_recv()
-        total = two(layer, far, lane) + yrecv[layer, far].astype(F32)
-        for k in range(1, lanes):
-            z = peer(k)
-            z_copy(layer, far, z).wait_recv()
-            total = total + zrecv[layer, z].astype(F32)
+        total = summed(far)
+        for slot in (far, near_z):
+            z_copy(layer, far, far, slot).wait_recv()
+            total = total + zrecv[layer, slot].astype(F32)
         return total
 
     def gathered(layer):
@@ -379,58 +376,75 @@
         ref = gathered(layer).at[rows_at(core, z, y)]
         return to(device, ref, ref, send, g_recv.at[layer, 2 * z + y])
 
-    def z_piece(layer, z, owner):
-        return piece_copy(layer, owner, lane, at_far(z), g_send.at[layer, z])
+    def z_piece(layer, owner, device):
+        return piece_copy(layer, owner, lane, at_far(device), g_send.at[layer])
 
     def y_piece(layer, z, y):
-        return piece_copy(layer, z, y, beside, b_send.at[layer, z])
+        return piece_copy(layer, z, y, beside, b_send.at[layer])
 
     def core_piece(layer, z, y, c):
         ref = gathered(layer).at[rows_at(c, z, y)]
-        return to(sibling, ref, ref, h_send.at[layer, 2 * z + y], h_recv.at[layer, 2 * z + y])
+        return to(sibling, ref, ref, h_send.at[layer], h_recv.at[layer])
 
     def gather(layer, then):
-        def send_z(k, _):
-            z_piece(layer, peer(k), far).start()
-            return 0
-
-        lax.fori_loop(1, lanes, send_z, 0)
-        then(1)
+        z_piece(layer, far, over_z).start()
+        z_piece(layer, far, near_z).start()
+        if layer == 0:
+            then(1)
         y_piece(layer, far, lane).start()
         core_piece(layer, far, lane, core).start()
-
-        def pass_z(k, _):
-            z = peer(k)
-            z_piece(layer, far, z).wait_recv()
+        if layer:
+            then(1)
+        for z in (over_z, near_z, last_z):
+            z_piece(layer, z, near_z).wait_recv()
+            if z is over_z:
+                z_piece(layer, z, near_z).start()
             y_piece(layer, z, lane).start()
             core_piece(layer, z, lane, core).start()
-            then(1 + k)
-            return 0
-
-        lax.fori_loop(1, lanes, pass_z, 0)
-
-        def pass_y(k, _):
-            z = peer(jnp.where(k == 0, lanes, k))
+        for z in (far, over_z, near_z, last_z):
             y_piece(layer, z, 1 - lane).wait_recv()
             core_piece(layer, z, 1 - lane, core).start()
-            then(1 + lanes + k)
-            return 0
-
-        lax.fori_loop(0, lanes, pass_y, 0)
-
-        def land(k, _):
-            core_piece(layer, k // 2, lax.rem(k, 2), 1 - core).wait_recv()
-            return 0
-
-        lax.fori_loop(0, chips, land, 0)
+
+        ref = gathered(layer).at[rows_of((1 - core) * side, side, side)]
+        to(sibling, ref, ref, h_send.at[layer], h_recv.at[layer]).wait_recv()
 
     def dole(k):
         if isinstance(k, int) and k + 1 < len(own_cuts):
             hand_out(1, own_cuts[k], own_cuts[k + 1])
             pass_on(1, cross_cuts[k], cross_cuts[k + 1])
 
-    def rest(k):
-        return None
+    def drain_blocks(layer):
+        all_blocks(layer).wait_send()
+        ref = tall.at[layer, rows_of(f * tall_half, tall_half, 16)]
+        across(ref, ref, d_send.at[layer], d_recv.at[layer, 0]).wait_send()
+
+    def drain_sum(layer):
+        to(sibling, pair.at[layer], pair.at[layer], p_send.at[layer], p_recv.at[layer, 0]).wait_send()
+        three = zsend.at[layer, pl.ds(0, 3)]
+        to(sibling, three, three, s_send.at[layer], s_recv.at[layer, 0]).wait_send()
+        four = ysend.at[layer]
+        to(beside, four, four, y_send.at[layer], y_recv.at[layer, 0]).wait_send()
+
+    def drain_gather(layer):
+        three, four, eight = zsend.at[layer, pl.ds(0, 3)], ysend.at[layer], pair.at[layer]
+        to(sibling, three, three, g_send.at[layer], g_recv.at[layer, 0]).wait_send()
+        to(beside, four, four, b_send.at[layer], g_recv.at[layer, 0]).wait_send()
+        to(sibling, eight, eight, h_send.at[layer], h_recv.at[layer]).wait_send()
+
+    def settle(k):
+        if k == 0:
+            drain_blocks(0)
+            drain_blocks(1)
+        if k == 1:
+            drain_sum(0)
+            drain_gather(0)
+            for i in range(2):
+                wide_copy(2 + i).wait_send()
+                partial_copy(i).wait_send()
+            guest_in.wait_send()
+            guest_copy(beside, lane, core, 1).wait_send()
+            guest_copy(sibling, lane, core, 2).wait_send()
+            guest_copy(sibling, 1 - lane, core, 3).wait_send()
 
     for i in range(2):
         partial_copy(i).wait_recv()
@@ -451,56 +465,15 @@
     hide_two()
     collect(1)
     project(1)
-    total = reduce(1, rest)
+    total = reduce(1, settle)
     mixed[own, :] = (middle[...].astype(F32) + 0.5 * total).astype(BF16)
-    gather(1, rest)
-
-    wide_copy(0).wait_recv()
-    wide_copy(1).wait_recv()
-    for i in range(4):
+    gather(1, settle)
+
+    drain_sum(1)
+    drain_gather(1)
+    for i in range(2):
+        wide_copy(i).wait_recv()
         wide_copy(i).wait_send()
-    for i in range(2):
-        partial_copy(i).wait_send()
-    guest_in.wait_send()
-    guest_copy(beside, lane, core, 1).wait_send()
-    guest_copy(sibling, lane, core, 2).wait_send()
-    guest_copy(sibling, 1 - lane, core, 3).wait_send()
-    for layer in range(2):
-
-        def drain(k, _):
-            block_copy(layer, lax.rem(t + k, n_tp), t).wait_send()
-            return 0
-
-        lax.fori_loop(1, n_tp, drain, 0)
-
-        def drain_x(k, _):
-            tall_copy(layer, turn(f, k)).wait_send()
-            return 0
-
-        lax.fori_loop(0, per_half, drain_x, 0)
-        swap(layer, 0).wait_send()
-        swap(layer, 1).wait_send()
-
-        def drain_z(k, _):
-            z = lax.rem(far + k, lanes)
-            z_copy(layer, z, far).wait_send()
-            z_piece(layer, z, far).wait_send()
-            return 0
-
-        lax.fori_loop(1, lanes, drain_z, 0)
-
-        def drain_y(z, _):
-            y_copy(layer, z).wait_send()
-            y_piece(layer, z, lane).wait_send()
-            return 0
-
-        lax.fori_loop(0, lanes, drain_y, 0)
-
-        def drain_c(k, _):
-            core_piece(layer, k // 2, lax.rem(k, 2), core).wait_send()
-            return 0
-
-        lax.fori_loop(0, chips, drain_c, 0)
 
 
 def flush(*refs):
@@ -553,10 +526,9 @@
             vmem((2, lanes, piece, model), BF16),
             vmem((2, lanes, piece, model), BF16),
             vmem((piece, model), BF16),
-            dma((9,)), dma((4,)), dma((4,)), dma((2, n_tp)), dma((2, n_tp)), dma((6,)), dma((6,)),
-            dma((2, n_tp)), dma((2, n_tp)),
-            dma((2, 2)), dma((2, 2)), dma((2, lanes)), dma((2, lanes)), dma((2, lanes)), dma((2, lanes)),
-            dma((2, lanes)), dma((2, chips)), dma((2, lanes)), dma((2, chips)), dma((2, chips)),
+            dma((9,)), dma((4,)), dma((4,)), dma((2,)), dma((2, n_tp // 2)), dma((6,)), dma((6,)),
+            dma((2,)), dma((2,)), dma((2,)), dma((2, 2)), dma((2,)), dma((2, lanes)),
+            dma((2,)), dma((2, lanes)), dma((2,)), dma((2, chips)), dma((2,)), dma((2,)), dma((2,)),
         ],
         compiler_params=pltpu.CompilerParams(
             collective_id=0, has_side_effects=True, vmem_limit_bytes=54 * 1024 * 1024
@@ -588,7 +560,7 @@
         P("fs", "tp"),
     )
     tp = mesh.shape["tp"]
-    paired = mesh.shape["fs"] == 2 and tp % 16 == 0 and tp & (tp - 1) == 0
+    paired = mesh.shape["fs"] == 2 and tp // 4 == 4 and tp % 4 == 0
     return jax.shard_map(
         functools.partial(fused, tp) if paired else body,
         mesh=mesh,

time: 121 us -> 118 us (0.975)
  Pallas kernels: 120 us -> 117 us
    pallas_call x1, Pallas kernels: 116 us -> 113 us  [fused(): pl.pallas_call(functools.partial(kernel, n_tp), out_shape=(vmem(x.shape,...]
where the time goes in v4:
time: 118 us
  Pallas kernels  117 us (99%)
    pallas_call x1, Pallas kernels, fused(): pl.pallas_call(functools.partial(kernel, n_tp), out_shape=(vmem(x.shape,...  113 us
    pallas_call x1, Pallas kernels, fused(): pl.pallas_call(flush, out_shape=tuple((jax.ShapeDtypeStruct(v.shape, v.dt...  3.8 us

profile of v4, /device:TPU:0, one launch (start us, length us, event | category | flops | bytes accessed | tf_op | source)
XLA Modules:
  0.0 117.8 jit_solution(13723180757769000105)
XLA Ops:
  0.6 113.4 %hand_over.1 = (bf16[256,2048]{1,0:T(8,128)(2,1)S(1)}, bf16[352,2048]{1,0:T(8,128)(2,1)S(1)}, bf16[352,2048]{1,0:T(8,128)(2,1)S(1)}, bf16[352,2048]{1,0:T(8,128)...) custom-call(bf16[256,2048]{1,0:T(8,128)(2,1)} %x_hbm.1, ...), custom_call_target="tpu_custom_call" | custom-call | tf_op jit(solution)/shard_map/hand_over/pallas_call | solution.py:505
  114.0 3.8 %flush.1 = (bf16[256,2048]{1,0:T(8,128)(2,1)}, bf16[352,2048]{1,0:T(8,128)(2,1)}, bf16[352,2048]{1,0:T(8,128)(2,1)}, bf16[352,2048]{1,0:T(8,128)(2,1)}, bf16[352...) custom-call(bf16[256,2048]{1,0:T(8,128)(2,1)S(1)} %get-tuple-element.21.refs_0_, ...), custom_call_target="tpu_custom_call" | custom-call | tf_op jit(solution)/shard_map/flush/pallas_call | solution.py:538

commit v5 on v4

--- a/solution.py
+++ b/solution.py
@@ -67,7 +67,7 @@
     n_tp,
     x_hbm, gain1_hbm, gate1_hbm, up1_hbm, down1_hbm, gain2_hbm, gate2_hbm, up2_hbm, down2_hbm,
     mixed, gate1, up1, down1, gate2, up2, down2,
-    x, gain, wide, tall_in, tall, normed, guest, psend, precv, kept, hidden, part, pair,
+    x, gain, wide, tall_in, tall, normed, guest, psend, precv, kept, upright, hidden, part, pair,
     ysend, yrecv, zsend, zrecv, middle,
     in_sem, x_send, x_recv, d_send, d_recv, v_send, v_recv, a_send, a_recv, p_send, p_recv,
     y_send, y_recv, s_send, s_recv,
@@ -92,7 +92,7 @@
     per_half = n_tp // 2
     eighth = per_half // 8
     own_cuts = (2 * eighth, 5 * eighth, per_half)
-    cross_cuts = (0, 3 * eighth, per_half)
+    cross_cuts = (eighth, 4 * eighth, per_half)
     lanes = chips // 2
     far = chip // 2
     lane = lax.rem(chip, 2)
@@ -274,30 +274,37 @@
         return across(psend.at[i], precv.at[i], v_send.at[4 + i], v_recv.at[4 + i])
 
     for i in range(2):
-        psend[i] = times(guest[...], i, near).astype(BF16)
+        psend[i] = lax.dot_general(
+            served[i][:, near], guest[...], turned, preferred_element_type=F32
+        ).astype(BF16)
         partial_copy(i).start()
     cross_tall(1, 0, per_half)
     for i in (2, 3, 0, 1):
         wide_copy(i).start()
     pass_on(0, 4 * eighth, 6 * eighth)
     for i in range(2):
-        kept[i] = times(normed[0, :, near], i, near)
+        kept[i] = lax.dot_general(
+            served[i][:, near], normed[0, :, near], turned, preferred_element_type=F32
+        )
     pass_on(0, 6 * eighth, per_half)
 
-    def gated(rows, g, u):
-        hidden[rows, :] = (g / (1.0 + jnp.exp(-g)) * u).astype(BF16)
+    def gated(g, u):
+        return (g / (1.0 + jnp.exp(-g)) * u).astype(BF16)
 
     def hide_one():
         def one(k, _):
             rows = rows_of(k * 32, 32, 32)
-            gated(rows, kept[0, rows, :] + precv[0, rows, :].astype(F32),
-                  kept[1, rows, :] + precv[1, rows, :].astype(F32))
+            upright[rows, :] = gated(
+                kept[0, rows, :] + precv[0, rows, :].astype(F32),
+                kept[1, rows, :] + precv[1, rows, :].astype(F32),
+            )
             return 0
 
-        lax.fori_loop(0, tokens // 32, one, 0)
+        lax.fori_loop(0, width // 32, one, 0)
 
     def hide_two():
-        gated(slice(None), times(normed[1], 2, slice(None)), times(normed[1], 3, slice(None)))
+        whole = slice(None)
+        hidden[...] = gated(times(normed[1], 2, whole), times(normed[1], 3, whole))
 
     near_z = lax.bitwise_xor(far, 1)
     over_z = lax.bitwise_xor(far, 2)
@@ -330,7 +337,12 @@
     def project(layer):
         def rows_for(c):
             rows = rows_of(c * side, side, side)
-            p = jnp.dot(hidden[rows, :], down[layer][...], preferred_element_type=F32)
+            if layer:
+                p = jnp.dot(hidden[rows, :], down2[...], preferred_element_type=F32)
+            else:
+                p = lax.dot_general(
+                    upright[:, rows], down1[...], (((0,), (0,)), ((), ())), preferred_element_type=F32
+                )
             part[layer, rows, :] = p.astype(BF16)
 
         rows_for(1 - core)
@@ -515,9 +527,10 @@
             vmem((2, 2 * tall_half, col), BF16),
             vmem((2, tokens, model), BF16),
             vmem((tokens, depth), BF16),
-            vmem((2, tokens, width), BF16),
-            vmem((2, tokens, width), BF16),
-            vmem((2, tokens, width), F32),
+            vmem((2, width, tokens), BF16),
+            vmem((2, width, tokens), BF16),
+            vmem((2, width, tokens), F32),
+            vmem((width, tokens), BF16),
             vmem((tokens, width), BF16),
             vmem((2, tokens, model), BF16),
             vmem((2, side, model), BF16),

time: 118 us -> 117 us (level)
  no operation moved by 1% of the time
where the time goes in v5:
time: 117 us
  Pallas kernels  116 us (99%)
    pallas_call x1, Pallas kernels, fused(): pl.pallas_call(functools.partial(kernel, n_tp), out_shape=(vmem(x.shape,...  113 us
    pallas_call x1, Pallas kernels, fused(): pl.pallas_call(flush, out_shape=tuple((jax.ShapeDtypeStruct(v.shape, v.dt...  3.8 us

profile of v5, /device:TPU:0, one launch (start us, length us, event | category | flops | bytes accessed | tf_op | source)
XLA Modules:
  0.0 117.1 jit_solution(4408015747040735704)
XLA Ops:
  0.6 112.7 %hand_over.1 = (bf16[256,2048]{1,0:T(8,128)(2,1)S(1)}, bf16[352,2048]{1,0:T(8,128)(2,1)S(1)}, bf16[352,2048]{1,0:T(8,128)(2,1)S(1)}, bf16[352,2048]{1,0:T(8,128)...) custom-call(bf16[256,2048]{1,0:T(8,128)(2,1)} %x_hbm.1, ...), custom_call_target="tpu_custom_call" | custom-call | tf_op jit(solution)/shard_map/hand_over/pallas_call | solution.py:517
  113.3 3.8 %flush.1 = (bf16[256,2048]{1,0:T(8,128)(2,1)}, bf16[352,2048]{1,0:T(8,128)(2,1)}, bf16[352,2048]{1,0:T(8,128)(2,1)}, bf16[352,2048]{1,0:T(8,128)(2,1)}, bf16[352...) custom-call(bf16[256,2048]{1,0:T(8,128)(2,1)S(1)} %get-tuple-element.21.refs_0_, ...), custom_call_target="tpu_custom_call" | custom-call | tf_op jit(solution)/shard_map/flush/pallas_call | solution.py:551
